TPU v7x, 256 devices: a whole 4x4x8 slice. The times are simulated.
256 devices in a mesh: ep: 64 (over z, y, core), tp: 4 (over x).
Axes of the slice: x: 4, y: 4, z: 8, core: 2. Of those that a mesh axis runs over, the one named last changes fastest.
Arguments:
- outer_gate: bfloat16 [32768, 2048], P('ep', 'tp'), may hold values from -6 to 6
- inner_gate: bfloat16 [32768, 2048], P('ep', 'tp'), may hold values from -6 to 6
- conv_values: bfloat16 [32768, 2048], P('ep', 'tp'), may hold values from -6 to 6
- conv_taps: bfloat16 [3, 2048], P(None, 'tp'), may hold values from -3 to 3
- out_weight: bfloat16 [2048, 2048], P('tp'), may hold values from -0.125 to 0.125
- moe_input: bfloat16 [32768, 2048], P(('ep', 'tp')), may hold values from -6 to 6
- norm_gain: bfloat16 [2048], replicated, may hold values from 0.099609375 to 1.8984375
- gate_proj: bfloat16 [64, 2048, 1024], P('ep', None, 'tp'), may hold values from -0.125 to 0.125
- up_proj: bfloat16 [64, 2048, 1024], P('ep', None, 'tp'), may hold values from -0.125 to 0.125
- down_proj: bfloat16 [64, 1024, 2048], P('ep', 'tp'), may hold values from -0.1875 to 0.1875
- shared_gate: bfloat16 [2048, 1024], P(None, 'tp'), may hold values from -0.125 to 0.125
- shared_up: bfloat16 [2048, 1024], P(None, 'tp'), may hold values from -0.125 to 0.125
- shared_down: bfloat16 [1024, 2048], P('tp'), may hold values from -0.1875 to 0.1875
- routes: int32 [32768, 2], P('ep'), may hold values from 0 to 63, all different within a row; in each aligned block of 128 rows (0 to 127, 128 to 255, ...) at most 8 rows name the same one
- route_weight: float32 [32768, 2], P('ep'), may hold values from 0.3 to 1.5
Outputs:
- mixer_out: bfloat16 [32768, 2048], P(('ep', 'tp'))
- expert_mix: bfloat16 [32768, 2048], P(('ep', 'tp'))
Inputs may be any that keep to these rules, and one draw needn't show every extreme that they name: `routes`: each row names 2 different experts. In the 128 rows of one device no expert is named more than 8 times, and in every draw some expert is named exactly 8 times in one device's rows.
All inputs are finite; a program needn't handle non-finite values.
Results may differ from a plain program's by a relative error of at most 0.012.
Values may be sent and summed in bfloat16 or wider, within the bound.
A program may use at most 128 MiB of HBM per device.

v0:
```python
from functools import partial
import jax
import jax.numpy as jnp
from jax import lax
from jax.sharding import PartitionSpec as P

epsilon = 1e-06


def shifted(block, axis, distance):
    devices = range(lax.axis_size(axis))
    route = [(i - distance, i) for i in devices if i - distance in devices]
    return lax.ppermute(block, axis, route)


def from_everyone(array, axis):
    length = lax.axis_size(axis)
    return lax.all_to_all(
        jnp.broadcast_to(array[None], (length, *array.shape)), axis, 0, 0, tiled=True
    )


def joined_along(blocks, dim):
    shape = list(blocks.shape[1:])
    shape[dim] *= blocks.shape[0]
    return jnp.moveaxis(blocks, 0, dim).reshape(shape)


def collect(array, axis, dim):
    blocks = from_everyone(array, axis)
    return joined_along(blocks, dim)


def gather_turned(arrays, axis, dims):
    turned = [jnp.moveaxis(a, dim, 0) for a, dim in zip(arrays, dims)]
    both = jnp.concatenate([t.reshape(len(t), -1) for t in turned], axis=1)
    result, at, outs = (lax.all_gather(both, axis, axis=0, tiled=True), 0, [])
    for t, dim in zip(turned, dims):
        share = result[:, at : at + t[0].size].reshape(-1, *t.shape[1:])
        outs.append(jnp.moveaxis(share, 0, dim))
        at += t[0].size
    return tuple(outs)


def rms_norm(inputs, scales):
    values = inputs.astype(jnp.float32)
    square = jnp.mean(values * values, axis=-1, keepdims=True)
    return (values * lax.rsqrt(square + epsilon) * scales.astype(jnp.float32)).astype(jnp.bfloat16)


def swiglu(inputs, gate_w, up_w):
    gate_term = jnp.dot(inputs, gate_w, preferred_element_type=jnp.float32)
    upward = jnp.dot(inputs, up_w, preferred_element_type=jnp.float32)
    return (jax.nn.silu(gate_term) * upward).astype(jnp.bfloat16)


def slot_table(block_routes, experts, capacity):
    flat_ids = block_routes.reshape(-1)
    onehot = (flat_ids[:, None] == jnp.arange(experts, dtype=jnp.int32)[None, :]).astype(jnp.int32)
    earlier = jnp.cumsum(onehot, axis=0) - onehot
    slot_ids = jnp.sum(earlier * onehot, axis=1)
    targets = flat_ids * capacity + slot_ids
    owners = jnp.arange(flat_ids.shape[0], dtype=jnp.int32) // block_routes.shape[1]
    sources = jnp.zeros((experts * capacity,), jnp.int32).at[targets].set(owners)
    filled = jnp.zeros((experts * capacity,), jnp.bfloat16).at[targets].set(1.0)
    return (sources, filled, targets)


def send_own(normed, own_routes, table_maker, ep_count, capacity):
    sources, filled, own_targets = table_maker(own_routes)
    outgoing = (normed[sources] * filled[:, None]).reshape(ep_count, capacity, normed.shape[1])
    landed = lax.all_to_all(outgoing, "ep", split_axis=0, concat_axis=0, tiled=True)
    return (landed, own_targets)


def per_device(
    outer_gate,
    inner_gate,
    conv_values,
    conv_taps,
    out_weight,
    moe_input,
    norm_gain,
    gate_proj,
    up_proj,
    down_proj,
    shared_gate,
    shared_up,
    shared_down,
    routes,
    route_weight,
):
    tp_count = lax.axis_size("tp")
    ep_count = lax.axis_size("ep")
    my_slot = lax.axis_index("tp")
    group_len = inner_gate.shape[0]
    mix_rows = group_len // tp_count
    channels = inner_gate.shape[1]
    model_width = moe_input.shape[1]
    own_rows = moe_input.shape[0]
    top_count = routes.shape[1]
    capacity = 2 * own_rows * top_count // ep_count
    slot_rows = ep_count * capacity
    reach_rows = conv_taps.shape[0] - 1
    edge_rows = jnp.stack(
        (inner_gate[group_len - reach_rows :], conv_values[group_len - reach_rows :])
    )
    before = shifted(edge_rows, "ep", 1)
    full_gate = jnp.concatenate((before[0], inner_gate), axis=0).astype(jnp.float32)
    full_values = jnp.concatenate((before[1], conv_values), axis=0).astype(jnp.float32)
    product = full_gate * full_values
    tap_values = conv_taps.astype(jnp.float32)
    convolved = tap_values[0] * product[0:group_len]
    for offset in range(1, reach_rows + 1):
        convolved = convolved + tap_values[offset] * product[offset : offset + group_len]
    gate_rows = (outer_gate.astype(jnp.float32) * convolved).astype(jnp.bfloat16)
    gate_rows = gate_rows.reshape(tp_count, mix_rows, channels)
    normed = rms_norm(moe_input, norm_gain)
    group_normed = collect(normed, "tp", 0)
    group_split = group_normed.reshape(tp_count, own_rows, model_width)
    own_weights = lax.dynamic_slice_in_dim(route_weight, my_slot * own_rows, own_rows, 0)
    own_routes = lax.dynamic_slice_in_dim(routes, my_slot * own_rows, own_rows, 0)
    table_maker = partial(slot_table, experts=ep_count, capacity=capacity)
    local_routed = None
    landed, own_targets = send_own(normed, own_routes, table_maker, ep_count, capacity)
    gate_full, up_full, down_full = gather_turned((gate_proj, up_proj, down_proj), "tp", (2, 2, 1))
    hidden = swiglu(landed.reshape(slot_rows, model_width), gate_full[0], up_full[0])
    unit_block = hidden.shape[1] // tp_count
    local_routed = jnp.zeros((slot_rows, model_width), jnp.float32)
    for piece_idx in range(tp_count):
        partial_sum = jnp.dot(
            hidden[:, piece_idx * unit_block : (piece_idx + 1) * unit_block],
            down_full[0, piece_idx * unit_block : (piece_idx + 1) * unit_block],
            preferred_element_type=jnp.float32,
        ).astype(jnp.bfloat16)
        local_routed = local_routed + partial_sum.astype(jnp.float32)
    routed_rows = 0
    expert_block = routed_rows + own_rows
    joint_block = mix_rows + expert_block
    dev_count = joint_block * lax.axis_size("tp") // joint_block
    block_rows = gate_rows
    block_rows = block_rows.reshape(dev_count * mix_rows, channels)
    projected = jnp.dot(block_rows, out_weight, preferred_element_type=jnp.float32)
    shared_in = group_split
    shared_in = shared_in.reshape(dev_count * own_rows, model_width)
    shared_out = jnp.dot(
        swiglu(shared_in, shared_gate, shared_up), shared_down, preferred_element_type=jnp.float32
    )
    shared_out = shared_out.reshape(dev_count, own_rows, model_width)
    combined = jnp.concatenate(
        (projected.reshape(dev_count, mix_rows, model_width), shared_out), axis=1
    )
    summed = lax.psum_scatter(
        combined.reshape(dev_count * joint_block, model_width).astype(jnp.bfloat16),
        "tp",
        scatter_dimension=0,
        tiled=True,
    ).astype(jnp.float32)
    mixer_out = summed[:mix_rows].astype(jnp.bfloat16)
    expert_total = summed[mix_rows:]
    routed_back = local_routed.astype(jnp.bfloat16)
    routed_back = routed_back.reshape(ep_count, capacity, model_width)
    returned = lax.all_to_all(routed_back, "ep", split_axis=0, concat_axis=0, tiled=True).reshape(
        slot_rows, model_width
    )
    picked = returned[own_targets].reshape(own_rows, top_count, model_width).astype(jnp.float32)
    routed = jnp.sum(picked * own_weights[:, :, None], axis=1)
    expert_mix = (expert_total + routed).astype(jnp.bfloat16)
    return (mixer_out, expert_mix)


def solution(mesh):
    return jax.shard_map(
        per_device,
        mesh=mesh,
        in_specs=(
            P("ep", "tp"),
            P("ep", "tp"),
            P("ep", "tp"),
            P(None, "tp"),
            P("tp", None),
            P(("ep", "tp"), None),
            P(),
            P("ep", None, "tp"),
            P("ep", None, "tp"),
            P("ep", "tp", None),
            P(None, "tp"),
            P(None, "tp"),
            P("tp", None),
            P("ep", None),
            P("ep", None),
        ),
        out_specs=(P(("ep", "tp"), None), P(("ep", "tp"), None)),
        check_vma=False,
    )
```

profile of v0, /device:TPU:8, one launch (start us, length us, event | category | flops | bytes accessed | tf_op | source)
XLA Modules:
  0.0 245.1 jit_solution(8007941486165297258)
XLA Ops:
  7.2 1.6 copy.24
  8.9 2.3 copy.25
  11.1 3.0 %pad_maximum_fusion.1 = bf16[256,6144]{1,0:T(8,128)(2,1)} fusion(bf16[256,2048]{1,0:T(8,128)(2,1)} %bitcast.97, bf16[256,2048]{1,0:T(8,128)(2,1)} %bitcast.94, bf16[256,2048]{1,0:T(8,128)(2,1)S(1)} %bitcast.93), kind=kLoop, calls=%fused_computation.11 | loop fusion | flops 9437184 | bytes 6291456 | tf_op jit(solution)/shard_map/concatenate | solution.py:36
  14.1 0.7 copy-done.9
  14.8 0.4 copy-done.2
  15.2 0.2 fusion.8
  15.4 0.2 fusion.10
  15.6 1.6 broadcast_in_dim.8
  17.2 4.5 %all-to-all-start = ((bf16[4,128,2048]{2,1,0:T(8,128)(2,1)}), bf16[4,128,2048]{2,1,0:T(8,128)(2,1)}, u32[]{:S(2)}, u32[]{:S(2)}) async-start(bf16[4,128,2048]{2,1,0:T(8,128)(2,1)} %broadcast_in_dim.8), calls=%async_computation | async-start | bytes 4194304 | tf_op jit(solution)/shard_map/all_to_all | solution.py:18
  21.7 0.7 broadcast_multiply_fusion
  22.5 0.1 eq.29
  22.6 0.1 eq.25
  22.8 0.6 reduce-window.6
  23.4 0.2 slice_reduce_fusion
  23.7 0.1 mul.132
  24.0 1.4 scatter_custom_fusion
  25.4 3.3 %gather_fusion = bf16[512,2048]{1,0:T(8,128)(2,1)} fusion(bf16[128,2048]{1,0:T(8,128)(2,1)S(1)} %fusion.10, s32[1024]{0:T(1024)S(1)} %pad_clamp_fusion.1), kind=kCustom, calls=%fused_computation | custom fusion | bytes 4196352 | tf_op jit(solution)/shard_map/gather | solution.py:71
  28.7 2.2 scatter_custom_fusion.1
  31.0 3.5 %bitcast_multiply_fusion = bf16[64,8,2048]{2,1,0:T(8,128)(2,1)} fusion(bf16[512,2048]{1,0:T(8,128)(2,1)} %gather_fusion, bf16[64,8]{1,0:T(8,128)(2,1)S(1)} %mul.134), kind=kLoop, calls=%fused_computation.21 | loop fusion | flops 1048576 | bytes 4195328 | tf_op jit(solution)/shard_map/mul | solution.py:71
  34.5 26.7 %all-to-all-done = bf16[4,128,2048]{2,1,0:T(8,128)(2,1)} async-done(((bf16[4,128,2048]{2,1,0:T(8,128)(2,1)}), bf16[4,128,2048]{2,1,0:T(8,128)(2,1)}, u32[]{:S(2)}, u32[]{:S(2)}) %all-to-all-start) | async-done | bytes 2097184 | tf_op jit(solution)/shard_map/all_to_all | solution.py:18
  61.2 13.8 %all-to-all-start.1 = ((bf16[64,8,2048]{2,1,0:T(8,128)(2,1)}), bf16[64,8,2048]{2,1,0:T(8,128)(2,1)}, u32[]{:S(2)}, u32[]{:S(2)}) async-start(bf16[64,8,2048]{2,1,0:T(8,128)(2,1)} %bitcast_multiply_fusion), calls=%async_computation.2 | async-start | bytes 4194304 | tf_op jit(solution)/shard_map/all_to_all | solution.py:72
  75.1 2.3 collective-permute-start
  77.5 3.1 %collective-permute-done = bf16[2,2,512]{2,1,0:T(2,128)(2,1)S(1)} collective-permute-done((bf16[2,2,512]{2,1,0:T(2,128)(2,1)S(1)}, bf16[2,2,512]{2,1,0:T(2,128)(2,1)S(1)}, u32[]{:S(2)}, u32[]{:S(2)}) %collective-permute-start) | collective-permute-done | bytes 4128 | tf_op jit(solution)/shard_map/ppermute | solution.py:13
  80.6 0.2 convert_multiply_fusion.2
  80.9 2.8 %convolution_convert_fusion.5 = bf16[512,2048]{1,0:T(8,128)(2,1)} fusion(bf16[512,2048]{1,0:T(8,128)(2,1)S(1)} %copy-done, f32[514,512]{1,0:T(8,128)S(1)} %convert_multiply_fusion.2, bf16[512,512]{1,0:T(8,128)(2,1)S(1)} %copy-done.12, f32[512]{0:T(512)S(1)} %bitcast.104, f32[512]{0:T(512)S(1)} %bitcast.103, f32[512]{0:T(512)S(1)} %bitcast.102), kind=kOutput, calls=%fused_computation.17 | convolution fusion | flops 1076887552 | bytes 7870464 | tf_op jit(solution)/shard_map/dot_general | solution.py:143
  83.6 3.2 %fusion.39 = f32[512,256]{1,0:T(8,128)} fusion(bf16[512,2048]{1,0:T(8,128)(2,1)} %bitcast.8, bf16[2048,256]{1,0:T(8,128)(2,1)S(1)} %copy-done.10), kind=kOutput, calls=%fused_computation.89 | convolution fusion | flops 536870912 | bytes 3670016 | tf_op jit(solution)/shard_map/dot_general | solution.py:52
  86.9 5.8 %convolution_convert_fusion.4 = bf16[512,2048]{1,0:T(8,128)(2,1)} fusion(bf16[256,2048]{1,0:T(8,128)(2,1)S(1)} %copy-done.11, bf16[512,2048]{1,0:T(8,128)(2,1)} %bitcast.8, bf16[2048,256]{1,0:T(8,128)(2,1)} %param.26, f32[512,256]{1,0:T(8,128)} %fusion.39), kind=kOutput, calls=%fused_computation.16 | convolution fusion | flops 1075576832 | bytes 6815744 | tf_op jit(solution)/shard_map/dot_general | solution.py:146
  92.7 4.2 %pad_maximum_fusion = bf16[4,256,2048]{2,1,0:T(8,128)(2,1)} fusion(bf16[4,128,2048]{2,1,0:T(8,128)(2,1)} %bitcast.96, bf16[4,128,2048]{2,1,0:T(8,128)(2,1)S(1)} %bitcast.95), kind=kLoop, calls=%fused_computation.9 | loop fusion | flops 8388608 | bytes 8388608 | tf_op jit(solution)/shard_map/concatenate | solution.py:150
  96.9 29.3 %all-to-all-done.1 = bf16[64,8,2048]{2,1,0:T(8,128)(2,1)} async-done(((bf16[64,8,2048]{2,1,0:T(8,128)(2,1)}), bf16[64,8,2048]{2,1,0:T(8,128)(2,1)}, u32[]{:S(2)}, u32[]{:S(2)}) %all-to-all-start.1) | async-done | bytes 2097184 | tf_op jit(solution)/shard_map/all_to_all | solution.py:72
  126.1 23.3 %all-gather.2.cloned.1.call-done = bf16[1024,6144]{1,0:T(8,128)(2,1)} async-done(((bf16[256,6144]{1,0:T(8,128)(2,1)}), bf16[1024,6144]{1,0:T(8,128)(2,1)}) %all-gather.2.cloned.1.call-update) | async-done | bytes 12582928 | tf_op jit(solution)/shard_map/all_gather | solution.py:37
  149.4 5.3 %fusion.1 = f32[512,1024]{1,0:T(8,128)S(1)} fusion(bf16[1024,6144]{1,0:T(8,128)(2,1)} %all-gather.2.cloned.1.call-done, bf16[64,8,2048]{2,1,0:T(8,128)(2,1)} %all-to-all-done.1), kind=kOutput, calls=%fused_computation.8 | convolution fusion | flops 2147483648 | bytes 8388608 | tf_op jit(solution)/shard_map/dot_general | solution.py:52
  154.7 1.1 copy-done.4
  155.8 0.6 slice_bitcast_fusion
  156.4 4.1 %multiply_convert_fusion = bf16[512,1024]{1,0:T(8,128)(2,1)S(1)} fusion(f32[512,1024]{1,0:T(8,128)S(1)} %fusion.1, bf16[1024,6144]{1,0:T(8,128)(2,1)S(1)} %copy-done.4, bf16[64,8,2048]{2,1,0:T(8,128)(2,1)} %all-to-all-done.1), kind=kOutput, calls=%fused_computation.23 | convolution fusion | flops 2150629376 | bytes 9437184 | tf_op jit(solution)/shard_map/dot_general | solution.py:53
  160.5 0.7 convolution_convert_fusion.2
  161.3 0.7 convolution_convert_fusion.1
  162.0 0.7 convolution_convert_fusion
  162.7 2.6 %fusion.2 = bf16[64,8,2048]{2,1,0:T(8,128)(2,1)} fusion(bf16[512,2048]{1,0:T(8,128)(2,1)S(1)} %convolution_convert_fusion, bf16[512,2048]{1,0:T(8,128)(2,1)S(1)} %convolution_convert_fusion.1, bf16[512,2048]{1,0:T(8,128)(2,1)S(1)} %convolution_convert_fusion.2, bf16[1,1024,2048]{2,1,0:T(8,128)(2,1)S(1)} %slice_bitcast_fusion, ...), kind=kOutput, calls=%fused_computation.18 | convolution fusion | flops 546308096 | bytes 9699328 | tf_op jit(solution)/shard_map/dot_general | solution.py:131
  165.4 12.1 %all-to-all-start.2 = ((bf16[64,8,2048]{2,1,0:T(8,128)(2,1)}), bf16[64,8,2048]{2,1,0:T(8,128)(2,1)S(1)}, u32[]{:S(2)}, u32[]{:S(2)}) async-start(bf16[64,8,2048]{2,1,0:T(8,128)(2,1)} %fusion.2), calls=%async_computation.3 | async-start | bytes 4194304 | tf_op jit(solution)/shard_map/all_to_all | solution.py:163
  177.5 0.7 constant_dynamic-slice_fusion
  178.1 0.1 copy.26
  178.3 24.4 %reduce-scatter.2.cloned.1.call-done = bf16[256,2048]{1,0:T(8,128)(2,1)} async-done(((bf16[1024,2048]{1,0:T(8,128)(2,1)}), bf16[256,2048]{1,0:T(8,128)(2,1)}) %reduce-scatter.2.cloned.1.call-update) | async-done | bytes 1048592 | tf_op jit(solution)/shard_map/reduce_scatter | solution.py:153
  202.7 1.9 slice.117
  204.5 24.2 %all-to-all-done.2 = bf16[64,8,2048]{2,1,0:T(8,128)(2,1)S(1)} async-done(((bf16[64,8,2048]{2,1,0:T(8,128)(2,1)}), bf16[64,8,2048]{2,1,0:T(8,128)(2,1)S(1)}, u32[]{:S(2)}, u32[]{:S(2)}) %all-to-all-start.2) | async-done | bytes 2097184 | tf_op jit(solution)/shard_map/all_to_all | solution.py:163
  228.7 1.4 gather_fusion.1
  230.1 2.4 reshape.113
  232.4 4.9 %multiply_reduce_fusion = f32[128,2048]{1,0:T(8,128)S(1)} fusion(f32[128,2,2048]{2,1,0:T(2,128)} %reshape.113, f32[128,2]{1,0:T(8,128)S(1)} %copy.26), kind=kLoop, calls=%fused_computation.22 | loop fusion | flops 786432 | bytes 3146752 | tf_op jit(solution)/shard_map/reduce_sum | solution.py:167
  237.3 0.9 add_convert_fusion.1
  (46 shorter events, 0.7 us)
Async XLA Ops:
  7.2 73.7 %copy-start = (bf16[512,2048]{1,0:T(8,128)(2,1)S(1)}, bf16[512,2048]{1,0:T(8,128)(2,1)}, u32[]{:S(2)}) copy-start(bf16[512,2048]{1,0:T(8,128)(2,1)} %param.19) | copy-start | bytes 6291460
  7.2 142.2 %all-gather.2.cloned.1.call-start = ((), (), s32[]{:S(2)}) async-start(), calls=%async_computation.5 | async-start | bytes 15728640 | tf_op jit(solution)/shard_map/all_gather | solution.py:37
  14.1 0.7 copy-start.9
  14.1 1.1 copy-start.2
  17.2 44.0 %all-to-all-start = ((bf16[4,128,2048]{2,1,0:T(8,128)(2,1)}), bf16[4,128,2048]{2,1,0:T(8,128)(2,1)}, u32[]{:S(2)}, u32[]{:S(2)}) async-start(bf16[4,128,2048]{2,1,0:T(8,128)(2,1)} %broadcast_in_dim.8), calls=%async_computation | async-start | bytes 4194304 | tf_op jit(solution)/shard_map/all_to_all | solution.py:18
  34.5 40.5 %copy-start.6 = (bf16[512,512]{1,0:T(8,128)(2,1)S(1)}, bf16[512,512]{1,0:T(8,128)(2,1)}, u32[]{:S(2)}) copy-start(bf16[512,512]{1,0:T(8,128)(2,1)} %param.16) | copy-start | bytes 1572868
  34.5 40.5 %copy-start.7 = (bf16[512,512]{1,0:T(8,128)(2,1)S(1)}, bf16[512,512]{1,0:T(8,128)(2,1)}, u32[]{:S(2)}) copy-start(bf16[512,512]{1,0:T(8,128)(2,1)} %param.17) | copy-start | bytes 1572868
  34.5 42.9 %copy-start.8 = (bf16[3,512]{1,0:T(4,128)(2,1)S(1)}, bf16[3,512]{1,0:T(4,128)(2,1)}, u32[]{:S(2)}) copy-start(bf16[3,512]{1,0:T(4,128)(2,1)} %param.18) | copy-start | bytes 9220
  61.2 65.0 %all-to-all-start.1 = ((bf16[64,8,2048]{2,1,0:T(8,128)(2,1)}), bf16[64,8,2048]{2,1,0:T(8,128)(2,1)}, u32[]{:S(2)}, u32[]{:S(2)}) async-start(bf16[64,8,2048]{2,1,0:T(8,128)(2,1)} %bitcast_multiply_fusion), calls=%async_computation.2 | async-start | bytes 4194304 | tf_op jit(solution)/shard_map/all_to_all | solution.py:72
  75.0 127.7 %reduce-scatter.2.cloned.1.call-start = ((), (), s32[]{:S(2)}) async-start(), calls=%async_computation.4 | async-start | bytes 5242880 | tf_op jit(solution)/shard_map/reduce_scatter | solution.py:153
  75.1 5.8 %copy-start.12 = (bf16[512,512]{1,0:T(8,128)(2,1)S(1)}, bf16[512,512]{1,0:T(8,128)(2,1)}, u32[]{:S(2)}) copy-start(bf16[512,512]{1,0:T(8,128)(2,1)} %param.15) | copy-start | bytes 1572868
  75.1 5.5 %collective-permute-start = (bf16[2,2,512]{2,1,0:T(2,128)(2,1)S(1)}, bf16[2,2,512]{2,1,0:T(2,128)(2,1)S(1)}, u32[]{:S(2)}, u32[]{:S(2)}) collective-permute-start(bf16[2,2,512]{2,1,0:T(2,128)(2,1)S(1)} %pad_maximum_fusion.2), channel_id=1, source_target_pairs={{0,4},{4,8},{8,12},{12,16},{16,20},{20,24},{24,28},{28,32},{32,36}... | collective-permute-start | bytes 12296 | tf_op jit(solution)/shard_map/ppermute | solution.py:13
  80.9 2.8 %copy-start.10 = (bf16[2048,256]{1,0:T(8,128)(2,1)S(1)}, bf16[2048,256]{1,0:T(8,128)(2,1)}, u32[]{:S(2)}) copy-start(bf16[2048,256]{1,0:T(8,128)(2,1)} %param.25) | copy-start | bytes 3145732
  83.6 3.2 %copy-start.11 = (bf16[256,2048]{1,0:T(8,128)(2,1)S(1)}, bf16[256,2048]{1,0:T(8,128)(2,1)}, u32[]{:S(2)}) copy-start(bf16[256,2048]{1,0:T(8,128)(2,1)} %param.27) | copy-start | bytes 3145732
  86.9 5.8 %copy-start.3 = (bf16[512,2048]{1,0:T(8,128)(2,1)S(1)}, bf16[512,2048]{1,0:T(8,128)(2,1)}, u32[]{:S(2)}) copy-start(bf16[512,2048]{1,0:T(8,128)(2,1)} %convolution_convert_fusion.5) | copy-start | bytes 6291460
  149.4 6.4 %copy-start.4 = (bf16[1024,6144]{1,0:T(8,128)(2,1)S(1)}, bf16[1024,6144]{1,0:T(8,128)(2,1)}, u32[]{:S(2)}) copy-start(bf16[1024,6144]{1,0:T(8,128)(2,1)} %all-gather.2.cloned.1.call-done) | copy-start | bytes 37748740
  165.4 63.3 %all-to-all-start.2 = ((bf16[64,8,2048]{2,1,0:T(8,128)(2,1)}), bf16[64,8,2048]{2,1,0:T(8,128)(2,1)S(1)}, u32[]{:S(2)}, u32[]{:S(2)}) async-start(bf16[64,8,2048]{2,1,0:T(8,128)(2,1)} %fusion.2), calls=%async_computation.3 | async-start | bytes 4194304 | tf_op jit(solution)/shard_map/all_to_all | solution.py:163
  230.1 8.2 %copy-start.1 = (bf16[512,2048]{1,0:T(8,128)(2,1)S(1)}, bf16[512,2048]{1,0:T(8,128)(2,1)}, u32[]{:S(2)}) copy-start(bf16[512,2048]{1,0:T(8,128)(2,1)} %param.19) | copy-start | bytes 6291460
  232.4 4.9 %copy-start.5 = (bf16[256,2048]{1,0:T(8,128)(2,1)S(1)}, bf16[256,2048]{1,0:T(8,128)(2,1)}, u32[]{:S(2)}) copy-start(bf16[256,2048]{1,0:T(8,128)(2,1)} %reduce-scatter.2.cloned.1.call-done) | copy-start | bytes 3145732
Sparse Core Ops, SparseCore 0:
  14.3 135.0 all-gather.1
  151.9 50.6 reduce-scatter.1
where the time goes:
time: 246 us; the launch traced here: 245 us
  waiting for transfers between devices  131 us (53%)
  starting transfers between devices  32.8 us (13%)
  matrix products  26.1 us (11%)
  local copies, waits for them, and re-layouts  22.4 us (9%)
  other arithmetic  18.6 us (8%)
  between operations  14.3 us (6%)
    all_to_all x1, waiting for transfers between devices, send_own(): lax.all_to_all(outgoing, 'ep', split_axis=0, concat_axis=0, tiled=True)  29.3 us
    all_to_all x1, waiting for transfers between devices, from_everyone(): lax.all_to_all(jnp.broadcast_to(array[None], (length, *array.shape)), axi...  26.7 us
    reduce_scatter x1, waiting for transfers between devices, per_device(): lax.psum_scatter(combined.reshape(dev_count * joint_block, model_width).a...  24.4 us
    all_to_all x1, waiting for transfers between devices, per_device(): lax.all_to_all(routed_back, 'ep', split_axis=0, concat_axis=0, tiled=True)  24.2 us
    all_gather x1, waiting for transfers between devices, gather_turned(): result, at, outs = (lax.all_gather(both, axis, axis=0, tiled=True), 0, [])  23.3 us
    all_to_all x1, starting transfers between devices, send_own(): lax.all_to_all(outgoing, 'ep', split_axis=0, concat_axis=0, tiled=True)  13.8 us
    all_to_all x1, starting transfers between devices, per_device(): lax.all_to_all(routed_back, 'ep', split_axis=0, concat_axis=0, tiled=True)  12.1 us
    dot_general x2, matrix products, swiglu(): gate_term = jnp.dot(inputs, gate_w, preferred_element_type=jnp.float32)  8.57 us
  transfers between devices with their start and end apart: 6, of which 6 were waited for; matrix products, arithmetic and copies ran while one was open for 20% of the time, Pallas kernels for 0%

commit v1 on v0

--- a/solution.py
+++ b/solution.py
@@ -34,7 +34,13 @@
 def gather_turned(arrays, axis, dims):
     turned = [jnp.moveaxis(a, dim, 0) for a, dim in zip(arrays, dims)]
     both = jnp.concatenate([t.reshape(len(t), -1) for t in turned], axis=1)
-    result, at, outs = (lax.all_gather(both, axis, axis=0, tiled=True), 0, [])
+    result, at, outs = (
+        jnp.concatenate(
+            lax.all_to_all(jnp.stack([both] * lax.axis_size(axis)), axis, 0, 0), axis=0
+        ),
+        0,
+        [],
+    )
     for t, dim in zip(turned, dims):
         share = result[:, at : at + t[0].size].reshape(-1, *t.shape[1:])
         outs.append(jnp.moveaxis(share, 0, dim))

time: 246 us -> 385 us (1.57)
  waiting for transfers between devices: 131 us -> 260 us
  local copies, waits for them, and re-layouts: 22.4 us -> 30.1 us
    all_to_all x0 -> x1, waiting for transfers between devices: none -> 150 us  [gather_turned(): lax.all_to_all(jnp.stack([both] * lax.axis_size(axis)), axis, 0, 0)]
    reduce_scatter x1, waiting for transfers between devices: 24.4 us -> 0.02 us  [per_device(): lax.psum_scatter(combined.reshape(dev_count * joint_block, model_width).a...]
    all_to_all x1, waiting for transfers between devices: 24.2 us -> 48.5 us  [per_device(): lax.all_to_all(routed_back, 'ep', split_axis=0, concat_axis=0, tiled=True)]
    all_gather x1 -> x0, waiting for transfers between devices: 23.3 us -> none  [gather_turned(): result, at, outs = (lax.all_gather(both, axis, axis=0, tiled=True), 0, [])]
    all_to_all x1, waiting for transfers between devices: 29.3 us -> 44.4 us  [send_own(): lax.all_to_all(outgoing, 'ep', split_axis=0, concat_axis=0, tiled=True)]
    all_to_all x1, waiting for transfers between devices: 26.7 us -> 14.3 us  [from_everyone(): lax.all_to_all(jnp.broadcast_to(array[None], (length, *array.shape)), axi...]
    another operation x1 -> x2, local copies, waits for them, and re-layouts: 0.01 us -> 7.94 us  [the longest x1 7.93 us: gather_turned(): jnp.stack([both] * lax.axis_size(axis))]
    all_to_all x0 -> x1, starting transfers between devices: none -> 6.46 us  [gather_turned(): lax.all_to_all(jnp.stack([both] * lax.axis_size(axis)), axis, 0, 0)]
  transfers between devices with their start and end apart: 6 -> 6, of which waited for: 6 -> 5; matrix products, arithmetic and copies ran while one was open for 20% -> 14% of each run, Pallas kernels for 0% -> 0%
where the time goes in v1:
time: 385 us
  waiting for transfers between devices  260 us (68%)
  starting transfers between devices  32.4 us (8%)
  local copies, waits for them, and re-layouts  30.1 us (8%)
  matrix products  26.9 us (7%)
  other arithmetic  21.1 us (5%)
  between operations  14.3 us (4%)
    all_to_all x1, waiting for transfers between devices, gather_turned(): lax.all_to_all(jnp.stack([both] * lax.axis_size(axis)), axis, 0, 0)  150 us
    all_to_all x1, waiting for transfers between devices, per_device(): lax.all_to_all(routed_back, 'ep', split_axis=0, concat_axis=0, tiled=True)  48.5 us
    all_to_all x1, waiting for transfers between devices, send_own(): lax.all_to_all(outgoing, 'ep', split_axis=0, concat_axis=0, tiled=True)  44.4 us
    all_to_all x1, waiting for transfers between devices, from_everyone(): lax.all_to_all(jnp.broadcast_to(array[None], (length, *array.shape)), axi...  14.3 us
    all_to_all x1, starting transfers between devices, send_own(): lax.all_to_all(outgoing, 'ep', split_axis=0, concat_axis=0, tiled=True)  12.3 us
    dot_general x2, matrix products, swiglu(): gate_term = jnp.dot(inputs, gate_w, preferred_element_type=jnp.float32)  8.38 us
    another operation x1, local copies, waits for them, and re-layouts, gather_turned(): jnp.stack([both] * lax.axis_size(axis))  7.93 us
  transfers between devices with their start and end apart: 6, of which 5 were waited for; matrix products, arithmetic and copies ran while one was open for 14% of the time, Pallas kernels for 0%

profile of v1, /device:TPU:8, one launch (start us, length us, event | category | flops | bytes accessed | tf_op | source)
XLA Modules:
  0.0 384.6 jit_solution(6951593752219085917)
XLA Ops:
  7.2 0.8 convert_element_type.85
  8.0 1.2 fusion.8
  9.3 1.2 fusion.10
  10.5 1.6 broadcast_in_dim.8
  12.1 4.5 %all-to-all-start = ((bf16[4,128,2048]{2,1,0:T(8,128)(2,1)}), bf16[4,128,2048]{2,1,0:T(8,128)(2,1)}, u32[]{:S(2)}, u32[]{:S(2)}) async-start(bf16[4,128,2048]{2,1,0:T(8,128)(2,1)} %broadcast_in_dim.8), calls=%async_computation | async-start | bytes 4194304 | tf_op jit(solution)/shard_map/all_to_all | solution.py:18
  16.6 0.7 broadcast_multiply_fusion
  17.3 0.1 copy.21
  17.4 0.1 eq.25
  17.6 0.1 eq.29
  17.8 0.1 mul.132
  18.0 0.6 reduce-window.6
  18.6 0.2 slice_reduce_fusion
  18.9 1.4 scatter_custom_fusion
  20.4 3.3 gather_fusion
  23.7 2.2 scatter_custom_fusion.1
  25.9 3.1 bitcast_multiply_fusion
  29.0 14.3 %all-to-all-done = bf16[4,128,2048]{2,1,0:T(8,128)(2,1)} async-done(((bf16[4,128,2048]{2,1,0:T(8,128)(2,1)}), bf16[4,128,2048]{2,1,0:T(8,128)(2,1)}, u32[]{:S(2)}, u32[]{:S(2)}) %all-to-all-start) | async-done | bytes 2097184 | tf_op jit(solution)/shard_map/all_to_all | solution.py:18
  43.3 12.3 %all-to-all-start.1 = ((bf16[64,8,2048]{2,1,0:T(8,128)(2,1)}), bf16[64,8,2048]{2,1,0:T(8,128)(2,1)}, u32[]{:S(2)}, u32[]{:S(2)}) async-start(bf16[64,8,2048]{2,1,0:T(8,128)(2,1)} %bitcast_multiply_fusion), calls=%async_computation.2 | async-start | bytes 4194304 | tf_op jit(solution)/shard_map/all_to_all | solution.py:78
  55.6 1.5 copy.25
  57.1 2.3 copy.24
  59.4 3.0 pad_maximum_fusion.1
  62.4 44.4 %all-to-all-done.1 = bf16[64,8,2048]{2,1,0:T(8,128)(2,1)} async-done(((bf16[64,8,2048]{2,1,0:T(8,128)(2,1)}), bf16[64,8,2048]{2,1,0:T(8,128)(2,1)}, u32[]{:S(2)}, u32[]{:S(2)}) %all-to-all-start.1) | async-done | bytes 2097184 | tf_op jit(solution)/shard_map/all_to_all | solution.py:78
  106.7 7.9 %stack.19 = bf16[4,256,6144]{2,1,0:T(8,128)(2,1)} broadcast(bf16[256,6144]{1,0:T(8,128)(2,1)} %pad_maximum_fusion.1), dimensions={1,2} | broadcast | bytes 15728640 | tf_op jit(solution)/shard_map/stack | solution.py:39
  114.7 6.5 %all-to-all-start.2 = ((bf16[4,256,6144]{2,1,0:T(8,128)(2,1)}), bf16[4,256,6144]{2,1,0:T(8,128)(2,1)}, u32[]{:S(2)}, u32[]{:S(2)}) async-start(bf16[4,256,6144]{2,1,0:T(8,128)(2,1)} %stack.19), calls=%async_computation.3 | async-start | bytes 25165824 | tf_op jit(solution)/shard_map/all_to_all | solution.py:39
  121.3 2.2 collective-permute-start
  123.5 2.8 collective-permute-done
  126.3 0.2 convert_multiply_fusion.2
  126.6 2.7 convolution_convert_fusion.5
  129.3 3.2 fusion.39
  132.5 5.8 %convolution_convert_fusion.4 = bf16[512,2048]{1,0:T(8,128)(2,1)} fusion(bf16[256,2048]{1,0:T(8,128)(2,1)S(1)} %copy-done.8, bf16[512,2048]{1,0:T(8,128)(2,1)} %bitcast.8, bf16[2048,256]{1,0:T(8,128)(2,1)} %param.26, f32[512,256]{1,0:T(8,128)} %fusion.39), kind=kOutput, calls=%fused_computation.16 | convolution fusion | flops 1075576832 | bytes 6815744 | tf_op jit(solution)/shard_map/dot_general | solution.py:152
  138.3 4.1 %pad_maximum_fusion = bf16[4,256,2048]{2,1,0:T(8,128)(2,1)} fusion(bf16[4,128,2048]{2,1,0:T(8,128)(2,1)} %bitcast.97, bf16[4,128,2048]{2,1,0:T(8,128)(2,1)S(1)} %bitcast.96), kind=kLoop, calls=%fused_computation.9 | loop fusion | flops 8388608 | bytes 8388608 | tf_op jit(solution)/shard_map/concatenate | solution.py:156
  142.5 149.9 %all-to-all-done.2 = bf16[4,256,6144]{2,1,0:T(8,128)(2,1)} async-done(((bf16[4,256,6144]{2,1,0:T(8,128)(2,1)}), bf16[4,256,6144]{2,1,0:T(8,128)(2,1)}, u32[]{:S(2)}, u32[]{:S(2)}) %all-to-all-start.2) | async-done | bytes 12582944 | tf_op jit(solution)/shard_map/all_to_all | solution.py:39
  292.4 5.2 %fusion.1 = f32[512,1024]{1,0:T(8,128)S(1)} fusion(bf16[1024,6144]{1,0:T(8,128)(2,1)} %bitcast.21, bf16[64,8,2048]{2,1,0:T(8,128)(2,1)} %all-to-all-done.1), kind=kOutput, calls=%fused_computation.8 | convolution fusion | flops 2147483648 | bytes 8388608 | tf_op jit(solution)/shard_map/dot_general | solution.py:58
  297.5 2.5 slice_bitcast_fusion
  300.0 5.3 %multiply_convert_fusion = bf16[512,1024]{1,0:T(8,128)(2,1)S(1)} fusion(f32[512,1024]{1,0:T(8,128)S(1)} %fusion.1, bf16[1024,6144]{1,0:T(8,128)(2,1)} %bitcast.21, bf16[64,8,2048]{2,1,0:T(8,128)(2,1)} %all-to-all-done.1), kind=kOutput, calls=%fused_computation.23 | convolution fusion | flops 2150629376 | bytes 9437184 | tf_op jit(solution)/shard_map/dot_general | solution.py:59
  305.4 0.7 convolution_convert_fusion
  306.1 0.7 convolution_convert_fusion.1
  306.8 0.7 convolution_convert_fusion.2
  307.5 2.6 fusion.2
  310.1 6.8 %all-to-all-start.3 = ((bf16[64,8,2048]{2,1,0:T(8,128)(2,1)}), bf16[64,8,2048]{2,1,0:T(8,128)(2,1)S(1)}, u32[]{:S(2)}, u32[]{:S(2)}) async-start(bf16[64,8,2048]{2,1,0:T(8,128)(2,1)} %fusion.2), calls=%async_computation.4 | async-start | bytes 4194304 | tf_op jit(solution)/shard_map/all_to_all | solution.py:169
  317.0 0.7 constant_dynamic-slice_fusion
  317.7 0.1 copy.26
  317.8 1.9 slice.117
  319.7 48.5 %all-to-all-done.3 = bf16[64,8,2048]{2,1,0:T(8,128)(2,1)S(1)} async-done(((bf16[64,8,2048]{2,1,0:T(8,128)(2,1)}), bf16[64,8,2048]{2,1,0:T(8,128)(2,1)S(1)}, u32[]{:S(2)}, u32[]{:S(2)}) %all-to-all-start.3) | async-done | bytes 2097184 | tf_op jit(solution)/shard_map/all_to_all | solution.py:169
  368.2 1.4 gather_fusion.1
  369.6 2.4 reshape.119
  372.0 4.9 %multiply_reduce_fusion = f32[128,2048]{1,0:T(8,128)S(1)} fusion(f32[128,2,2048]{2,1,0:T(2,128)} %reshape.119, f32[128,2]{1,0:T(8,128)S(1)} %copy.26), kind=kLoop, calls=%fused_computation.22 | loop fusion | flops 786432 | bytes 3146752 | tf_op jit(solution)/shard_map/reduce_sum | solution.py:173
  376.9 0.9 add_convert_fusion.1
  (40 shorter events, 0.6 us)
Async XLA Ops:
  7.2 119.4 %copy-start = (bf16[512,2048]{1,0:T(8,128)(2,1)S(1)}, bf16[512,2048]{1,0:T(8,128)(2,1)}, u32[]{:S(2)}) copy-start(bf16[512,2048]{1,0:T(8,128)(2,1)} %param.19) | copy-start | bytes 6291460
  12.1 31.2 %all-to-all-start = ((bf16[4,128,2048]{2,1,0:T(8,128)(2,1)}), bf16[4,128,2048]{2,1,0:T(8,128)(2,1)}, u32[]{:S(2)}, u32[]{:S(2)}) async-start(bf16[4,128,2048]{2,1,0:T(8,128)(2,1)} %broadcast_in_dim.8), calls=%async_computation | async-start | bytes 4194304 | tf_op jit(solution)/shard_map/all_to_all | solution.py:18
  43.3 63.5 %all-to-all-start.1 = ((bf16[64,8,2048]{2,1,0:T(8,128)(2,1)}), bf16[64,8,2048]{2,1,0:T(8,128)(2,1)}, u32[]{:S(2)}, u32[]{:S(2)}) async-start(bf16[64,8,2048]{2,1,0:T(8,128)(2,1)} %bitcast_multiply_fusion), calls=%async_computation.2 | async-start | bytes 4194304 | tf_op jit(solution)/shard_map/all_to_all | solution.py:78
  114.7 6.5 %copy-start.4 = (bf16[512,512]{1,0:T(8,128)(2,1)S(1)}, bf16[512,512]{1,0:T(8,128)(2,1)}, u32[]{:S(2)}) copy-start(bf16[512,512]{1,0:T(8,128)(2,1)} %param.16) | copy-start | bytes 1572868
  114.7 6.5 %copy-start.5 = (bf16[512,512]{1,0:T(8,128)(2,1)S(1)}, bf16[512,512]{1,0:T(8,128)(2,1)}, u32[]{:S(2)}) copy-start(bf16[512,512]{1,0:T(8,128)(2,1)} %param.17) | copy-start | bytes 1572868
  114.7 8.8 %copy-start.6 = (bf16[3,512]{1,0:T(4,128)(2,1)S(1)}, bf16[3,512]{1,0:T(4,128)(2,1)}, u32[]{:S(2)}) copy-start(bf16[3,512]{1,0:T(4,128)(2,1)} %param.18) | copy-start | bytes 9220
  114.7 177.7 %all-to-all-start.2 = ((bf16[4,256,6144]{2,1,0:T(8,128)(2,1)}), bf16[4,256,6144]{2,1,0:T(8,128)(2,1)}, u32[]{:S(2)}, u32[]{:S(2)}) async-start(bf16[4,256,6144]{2,1,0:T(8,128)(2,1)} %stack.19), calls=%async_computation.3 | async-start | bytes 25165824 | tf_op jit(solution)/shard_map/all_to_all | solution.py:39
  121.1 196.7 %reduce-scatter.2.cloned.1.call-start = ((), (), s32[]{:S(2)}) async-start(), calls=%async_computation.5 | async-start | bytes 5242880 | tf_op jit(solution)/shard_map/reduce_scatter | solution.py:159
  121.2 5.4 %copy-start.9 = (bf16[512,512]{1,0:T(8,128)(2,1)S(1)}, bf16[512,512]{1,0:T(8,128)(2,1)}, u32[]{:S(2)}) copy-start(bf16[512,512]{1,0:T(8,128)(2,1)} %param.15) | copy-start | bytes 1572868
  121.3 5.1 %collective-permute-start = (bf16[2,2,512]{2,1,0:T(2,128)(2,1)S(1)}, bf16[2,2,512]{2,1,0:T(2,128)(2,1)S(1)}, u32[]{:S(2)}, u32[]{:S(2)}) collective-permute-start(bf16[2,2,512]{2,1,0:T(2,128)(2,1)S(1)} %pad_maximum_fusion.2), channel_id=1, source_target_pairs={{0,4},{4,8},{8,12},{12,16},{16,20},{20,24},{24,28},{28,32},{32,36}... | collective-permute-start | bytes 12296 | tf_op jit(solution)/shard_map/ppermute | solution.py:13
  126.6 2.7 copy-start.7
  129.3 3.2 copy-start.8
  132.5 5.8 %copy-start.2 = (bf16[512,2048]{1,0:T(8,128)(2,1)S(1)}, bf16[512,2048]{1,0:T(8,128)(2,1)}, u32[]{:S(2)}) copy-start(bf16[512,2048]{1,0:T(8,128)(2,1)} %convolution_convert_fusion.5) | copy-start | bytes 6291460
  310.1 58.1 %all-to-all-start.3 = ((bf16[64,8,2048]{2,1,0:T(8,128)(2,1)}), bf16[64,8,2048]{2,1,0:T(8,128)(2,1)S(1)}, u32[]{:S(2)}, u32[]{:S(2)}) async-start(bf16[64,8,2048]{2,1,0:T(8,128)(2,1)} %fusion.2), calls=%async_computation.4 | async-start | bytes 4194304 | tf_op jit(solution)/shard_map/all_to_all | solution.py:169
  369.6 8.2 %copy-start.1 = (bf16[512,2048]{1,0:T(8,128)(2,1)S(1)}, bf16[512,2048]{1,0:T(8,128)(2,1)}, u32[]{:S(2)}) copy-start(bf16[512,2048]{1,0:T(8,128)(2,1)} %param.19) | copy-start | bytes 6291460
  372.0 4.9 %copy-start.3 = (bf16[256,2048]{1,0:T(8,128)(2,1)S(1)}, bf16[256,2048]{1,0:T(8,128)(2,1)}, u32[]{:S(2)}) copy-start(bf16[256,2048]{1,0:T(8,128)(2,1)} %reduce-scatter.2.cloned.1.call-done) | copy-start | bytes 3145732
Sparse Core Ops, SparseCore 0:
  142.6 81.4 reduce-scatter.1
